TPU v7x, 32 devices: a whole 2x2x4 slice. The times are simulated.
32 devices in a mesh: sp: 16 (over z, y, x), tp: 2 (over core).
Axes of the slice: x: 2, y: 2, z: 4, core: 2. Of those that a mesh axis runs over, the one named last changes fastest.
Arguments:
- residual: bfloat16 [6144, 2048], P('sp'), may hold values from -6 to 6
- queries: bfloat16 [6144, 2048], P('sp', 'tp'), may hold values from -48 to 48
- keys: bfloat16 [6144, 2048], P('sp', 'tp'), may hold values from -48 to 48
- values: bfloat16 [6144, 2048], P('sp', 'tp'), may hold values from -6 to 6
- gate_cache: float32 [6144, 32], P('sp', 'tp'), may hold values from -1544 to 0, as said below
- doc_ids: int32 [6144], P('sp'), may hold values from 0 to 7, never falling along the last dimension, each value on 1 to 1536 neighbouring positions
- out_weight: bfloat16 [2048, 2048], P('tp'), may hold values from -1 to 1
- mix_gain: float32 [2048], replicated, may hold values from 0.1 to 1.9
- gate_weight: bfloat16 [2048, 5120], P('sp', 'tp'), may hold values from -0.125 to 0.125
- up_weight: bfloat16 [2048, 5120], P('sp', 'tp'), may hold values from -0.125 to 0.125
- down_weight: bfloat16 [5120, 2048], P('tp', 'sp'), may hold values from -0.15625 to 0.15625
Outputs:
- layer_out: bfloat16 [6144, 2048], P(('sp', 'tp'))
Inputs may be any that keep to these rules, and one draw needn't show every extreme that they name: `doc_ids`: positions of one document are consecutive; each document has 1 to 1536 positions, and one has exactly that many. `gate_cache`: no column rises from one position to the next.
All inputs are finite; a program needn't handle non-finite values.
Results may differ from a plain program's by a relative error of at most 0.018.
Values may be sent and summed in bfloat16 or wider, within the bound.
A program may use at most 128 MiB of HBM per device.

v0:
```python
import jax
import jax.numpy as jnp
from jax import lax
from jax.sharding import PartitionSpec as P

REACH = 4


EPSILON = 1e-06
NEGATIVE = -1e30


def from_behind(value, axis, steps):
    count = lax.axis_size(axis)
    first, last = (max(0, -steps), min(count, count - steps))
    return lax.ppermute(value, axis, [(source, source + steps) for source in range(first, last)])


def normalize(middle, gain):
    widened = middle.astype(jnp.float32)
    factor = lax.rsqrt(jnp.mean(widened * widened, axis=-1, keepdims=True) + EPSILON)
    return (widened * factor * gain).astype(jnp.bfloat16)


def local(
    residual,
    queries,
    keys,
    values,
    gate_cache,
    doc_ids,
    out_weight,
    mix_gain,
    gate_weight,
    up_weight,
    down_weight,
):
    tok_rows = queries.shape[0]
    heads_here = gate_cache.shape[1]
    head_size = queries.shape[1] // heads_here
    sp_index = lax.axis_index("sp")
    key_parts = [keys]
    value_parts = [values]
    cache_parts = [gate_cache]
    doc_parts = [doc_ids]
    for distance in range(1, REACH + 1):
        moved_keys, moved_values = from_behind((keys, values), "sp", distance)
        moved_cache, moved_docs = from_behind((gate_cache, doc_ids), "sp", distance)
        key_parts.append(moved_keys)
        value_parts.append(moved_values)
        cache_parts.append(moved_cache)
        doc_parts.append(moved_docs)
    all_keys = jnp.concatenate(key_parts[::-1], axis=0)
    all_values = jnp.concatenate(value_parts[::-1], axis=0)
    all_cache = jnp.concatenate(cache_parts[::-1], axis=0)
    all_docs = jnp.concatenate(doc_parts[::-1], axis=0)
    key_count = all_keys.shape[0]
    query_pos = sp_index * tok_rows + jnp.arange(tok_rows, dtype=jnp.int32)
    key_pos = (sp_index - REACH) * tok_rows + jnp.arange(key_count, dtype=jnp.int32)
    visible = (
        (key_pos[None, :] <= query_pos[:, None])
        & (key_pos[None, :] >= 0)
        & (all_docs[None, :] == doc_ids[:, None])
    )
    query_heads = queries.reshape(tok_rows, heads_here, head_size)
    key_heads = all_keys.reshape(key_count, heads_here, head_size)
    value_heads = all_values.reshape(key_count, heads_here, head_size)
    score_scale = head_size ** (-0.5)
    scores = (
        jnp.einsum("qhd,khd->hqk", query_heads, key_heads, preferred_element_type=jnp.float32)
        * score_scale
    )
    scores = scores + gate_cache.T[:, :, None] - all_cache.T[:, None, :]
    scores = jnp.where(visible[None], scores, NEGATIVE)
    row_max = jnp.max(scores, axis=-1, keepdims=True)
    exp_scores = jnp.exp(scores - row_max)
    weights = (exp_scores / jnp.sum(exp_scores, axis=-1, keepdims=True)).astype(jnp.bfloat16)
    attended = jnp.einsum("hqk,khd->qhd", weights, value_heads, preferred_element_type=jnp.float32)
    attended = attended.astype(jnp.bfloat16).reshape(tok_rows, heads_here * head_size)
    row_share = tok_rows // lax.axis_size("tp")
    tp_index = lax.axis_index("tp")
    partial_value = jnp.dot(attended, out_weight, preferred_element_type=jnp.float32)
    attn_sum = lax.psum(partial_value.astype(jnp.bfloat16), "tp").astype(jnp.float32)
    whole_middle = (residual.astype(jnp.float32) + attn_sum).astype(jnp.bfloat16)
    mixer_in = normalize(whole_middle, mix_gain)
    middle = lax.dynamic_slice_in_dim(whole_middle, tp_index * row_share, row_share, 0)
    held_gate, held_up = (
        lax.all_gather(gate_weight, "sp", axis=0, tiled=True),
        lax.all_gather(up_weight, "sp", axis=0, tiled=True),
    )
    gate_proj = jnp.dot(mixer_in, held_gate, preferred_element_type=jnp.float32)
    up_proj = jnp.dot(mixer_in, held_up, preferred_element_type=jnp.float32)
    hidden = (jax.nn.silu(gate_proj) * up_proj).astype(jnp.bfloat16)
    partials = jnp.dot(
        hidden,
        lax.all_gather(down_weight, "sp", axis=1, tiled=True),
        preferred_element_type=jnp.float32,
    )
    down_sum = lax.psum_scatter(
        partials.astype(jnp.bfloat16), "tp", scatter_dimension=0, tiled=True
    ).astype(jnp.float32)
    return (middle.astype(jnp.float32) + down_sum).astype(jnp.bfloat16)


def solution(mesh):
    return jax.shard_map(
        local,
        mesh=mesh,
        in_specs=(
            P("sp", None),
            P("sp", "tp"),
            P("sp", "tp"),
            P("sp", "tp"),
            P("sp", "tp"),
            P("sp"),
            P("tp", None),
            P(),
            P("sp", "tp"),
            P("sp", "tp"),
            P("tp", "sp"),
        ),
        out_specs=P(("sp", "tp"), None),
        check_vma=False,
    )
```

profile of v0, /device:TPU:0, one launch (start us, length us, event | category | flops | bytes accessed | tf_op | source)
XLA Modules:
  0.0 706.5 jit_solution(17122347479193859977)
XLA Ops:
  7.4 5.1 collective-permute-start.4
  12.5 4.4 collective-permute-start.5
  16.8 3.4 collective-permute-start.6
  20.3 2.5 collective-permute-start.7
  22.8 3.5 collective-permute-start.8
  26.4 1.5 copy.18
  27.9 3.9 collective-permute-start.9
  31.8 3.4 collective-permute-start.10
  35.3 1.3 collective-permute-start.11
  36.6 1.8 collective-permute-start.12
  38.4 0.7 constant_dynamic-update-slice_fusion.16
  39.1 3.2 compare_and_fusion
  42.7 54.6 %collective-permute-start.13 = (f32[384,16]{0,1:T(8,128)}, f32[384,16]{0,1:T(8,128)S(1)}, u32[]{:S(2)}, u32[]{:S(2)}) collective-permute-start(f32[384,16]{0,1:T(8,128)} %param.15), channel_id=1, source_target_pairs={{0,6},{2,8},{4,10},{6,12},{8,14},{10,16},{12,18},{14,20},{16,22},{... | collective-permute-start | bytes 73736 | tf_op jit(solution)/shard_map/ppermute | solution.py:16
  97.3 1.7 collective-permute-done.13
  99.0 1.3 collective-permute-start.14
  100.3 1.7 collective-permute-done.14
  102.0 6.3 collective-permute-start.15
  108.3 1.7 collective-permute-done.15
  110.0 8.2 %collective-permute-start = (bf16[384,1024]{1,0:T(8,128)(2,1)}, bf16[384,1024]{1,0:T(8,128)(2,1)S(1)}, u32[]{:S(2)}, u32[]{:S(2)}) collective-permute-start(bf16[384,1024]{1,0:T(8,128)(2,1)} %param.14), channel_id=1, source_target_pairs={{0,8},{2,10},{4,12},{6,14},{8,16},{10,18},{12,20},{14,22},{16,24},... | collective-permute-start | bytes 2359304 | tf_op jit(solution)/shard_map/ppermute | solution.py:16
  118.3 0.7 constant_dynamic-update-slice_fusion.11
  119.0 3.1 collective-permute-start.1
  122.1 0.9 constant_dynamic-update-slice_fusion.10
  123.0 2.8 collective-permute-start.2
  125.8 1.0 constant_dynamic-update-slice_fusion.9
  126.8 2.8 collective-permute-start.3
  129.6 0.9 constant_dynamic-update-slice_fusion.8
  130.5 0.9 constant_dynamic-update-slice_fusion.7
  131.4 0.9 constant_dynamic-update-slice_fusion.6
  132.4 6.3 copy.17
  138.7 0.9 constant_dynamic-update-slice_fusion.4
  139.6 2.1 constant_dynamic-update-slice_fusion.3
  141.7 11.9 %collective-permute-done.2 = bf16[384,1024]{1,0:T(8,128)(2,1)S(1)} collective-permute-done((bf16[384,1024]{1,0:T(8,128)(2,1)S(1)}, bf16[384,1024]{1,0:T(8,128)(2,1)S(1)}, u32[]{:S(2)}, u32[]{:S(2)}) %collective-permute-start.2) | collective-permute-done | bytes 786464 | tf_op jit(solution)/shard_map/ppermute | solution.py:16
  153.7 0.9 constant_dynamic-update-slice_fusion.2
  154.6 2.1 constant_dynamic-update-slice_fusion.1
  156.7 0.9 constant_dynamic-update-slice_fusion
  157.6 6.4 copy.16
  164.1 26.9 %fusion.22 = (f32[16,384]{1,0:T(8,128)S(1)}, f32[16,384,1920]{1,2,0:T(8,128)}) fusion(f32[16,1920]{1,0:T(8,128)S(1)} %bitcast.33, f32[16,384]{1,0:T(8,128)S(1)} %bitcast.32, pred[384,1920]{0,1:T(8,128)(4,1)S(1)} %copy-done.3, bf16[1920,16,64]{0,2,1:T(8,128)(2,1)} %bitcast.29, bf16[384,16,64]{0,2,1:T(8,128)(2,1)S(1)} %bitcast.31), kind=kOutput, calls=%fused_computation.53 | convolution fusion | flops 1580730240 | bytes 52813824 | tf_op jit(solution)/shard_map/sub | solution.py:76
  190.9 17.4 %fusion.14 = bf16[16,64,384]{2,1,0:T(8,128)(2,1)S(1)} fusion(bf16[1920,16,64]{0,2,1:T(8,128)(2,1)} %bitcast.30, f32[16,384,1920]{1,2,0:T(8,128)} %get-tuple-element.8, f32[16,384]{1,0:T(8,128)S(1)} %get-tuple-element.7), kind=kOutput, calls=%fused_computation.24 | convolution fusion | flops 1533935616 | bytes 51929088 | tf_op jit(solution)/shard_map/hqk,khd->qhd/dot_general | solution.py:78
  208.3 3.0 convolution_convert_fusion
  213.4 43.0 %all-reduce.2.cloned.1.call-done = bf16[384,2048]{1,0:T(8,128)(2,1)} async-done(((bf16[384,2048]{1,0:T(8,128)(2,1)}), bf16[384,2048]{1,0:T(8,128)(2,1)}) %all-reduce.2.cloned.1.call-update) | async-done | bytes 1572880 | tf_op jit(solution)/shard_map/psum | solution.py:83
  256.3 2.1 fusion.11
  258.5 111.8 %all-gather.4.cloned.1.call-done = bf16[2048,2560]{1,0:T(8,128)(2,1)} async-done(((bf16[128,2560]{1,0:T(8,128)(2,1)}), bf16[2048,2560]{1,0:T(8,128)(2,1)}) %all-gather.4.cloned.1.call-update) | async-done | bytes 10485776 | tf_op jit(solution)/shard_map/all_gather | solution.py:88
  370.3 8.9 %fusion.17 = f32[384,2560]{1,0:T(8,128)} fusion(bf16[2048,2560]{1,0:T(8,128)(2,1)} %all-gather.4.cloned.1.call-done, bf16[384,2048]{1,0:T(8,128)(2,1)S(1)} %get-tuple-element.6, f32[2048]{0:T(1024)S(1)} %copy-done.6, f32[384]{0:T(512)S(1)} %add_rsqrt_fusion), kind=kOutput, calls=%fused_computation.25 | convolution fusion | flops 4029677568 | bytes 16000512 | tf_op jit(solution)/shard_map/dot_general | solution.py:91
  379.2 123.1 %all-gather.6.cloned.1.call-done = bf16[2048,2560]{1,0:T(8,128)(2,1)} async-done(((bf16[128,2560]{1,0:T(8,128)(2,1)}), bf16[2048,2560]{1,0:T(8,128)(2,1)}) %all-gather.6.cloned.1.call-update) | async-done | bytes 10485776 | tf_op jit(solution)/shard_map/all_gather | solution.py:89
  502.3 169.3 %all-gather.8.cloned.1.call-done = bf16[2560,2048]{1,0:T(8,128)(2,1)} async-done(((bf16[2560,128]{1,0:T(8,128)(2,1)}), bf16[2560,2048]{1,0:T(8,128)(2,1)}) %all-gather.8.cloned.1.call-update) | async-done | bytes 10485776 | tf_op jit(solution)/shard_map/all_gather | solution.py:96
  671.5 17.7 %convolution_convert_fusion.1 = bf16[384,2048]{1,0:T(8,128)(2,1)} fusion(bf16[2560,2048]{1,0:T(8,128)(2,1)} %all-gather.8.cloned.1.call-done, bf16[2048,2560]{1,0:T(8,128)(2,1)} %all-gather.6.cloned.1.call-done, f32[384,2560]{1,0:T(8,128)} %fusion.17, bf16[384,2048]{1,0:T(8,128)(2,1)S(1)} %get-tuple-element.6, f32[2048]{0:T(1024)S(1)} %copy-done.6, ...), kind=kOutput, calls=%fused_computation.22 | convolution fusion | flops 8062894080 | bytes 28059136 | tf_op jit(solution)/shard_map/dot_general | solution.py:94
  689.3 7.4 %reduce-scatter.2.cloned.1.call-done = bf16[192,2048]{1,0:T(8,128)(2,1)} async-done(((bf16[384,2048]{1,0:T(8,128)(2,1)}), bf16[192,2048]{1,0:T(8,128)(2,1)}) %reduce-scatter.2.cloned.1.call-update) | async-done | bytes 786448 | tf_op jit(solution)/shard_map/reduce_scatter | solution.py:99
  696.7 2.3 add_convert_fusion.1
  (49 shorter events, 2.4 us)
Async XLA Ops:
  7.4 115.6 %copy-start.2 = (bf16[384,1024]{1,0:T(8,128)(2,1)S(1)}, bf16[384,1024]{1,0:T(8,128)(2,1)}, u32[]{:S(2)}) copy-start(bf16[384,1024]{1,0:T(8,128)(2,1)} %param.14) | copy-start | bytes 2359300
  7.4 249.0 %all-reduce.2.cloned.1.call-start = ((), (), s32[]{:S(2)}) async-start(), calls=%async_computation.1 | async-start | bytes 3145728 | tf_op jit(solution)/shard_map/psum | solution.py:83
  7.4 20.5 %collective-permute-start.4 = (s32[384]{0:T(512)}, s32[384]{0:T(512)S(1)}, u32[]{:S(2)}, u32[]{:S(2)}) collective-permute-start(s32[384]{0:T(512)} %param.16), channel_id=1, source_target_pairs={{0,8},{2,10},{4,12},{6,14},{8,16},{10,18},{12,20},{14,22},{16,24},... | collective-permute-start | bytes 4616 | tf_op jit(solution)/shard_map/ppermute | solution.py:16
  12.5 19.4 %collective-permute-start.5 = (s32[384]{0:T(512)}, s32[384]{0:T(512)S(1)}, u32[]{:S(2)}, u32[]{:S(2)}) collective-permute-start(s32[384]{0:T(512)} %param.16), channel_id=1, source_target_pairs={{0,6},{2,8},{4,10},{6,12},{8,14},{10,16},{12,18},{14,20},{16,22},{... | collective-permute-start | bytes 4616 | tf_op jit(solution)/shard_map/ppermute | solution.py:16
  16.8 18.4 %collective-permute-start.6 = (s32[384]{0:T(512)}, s32[384]{0:T(512)S(1)}, u32[]{:S(2)}, u32[]{:S(2)}) collective-permute-start(s32[384]{0:T(512)} %param.16), channel_id=1, source_target_pairs={{0,4},{2,6},{4,8},{6,10},{8,12},{10,14},{12,16},{14,18},{16,20},{1... | collective-permute-start | bytes 4616 | tf_op jit(solution)/shard_map/ppermute | solution.py:16
  20.3 16.4 %collective-permute-start.7 = (s32[384]{0:T(512)}, s32[384]{0:T(512)S(1)}, u32[]{:S(2)}, u32[]{:S(2)}) collective-permute-start(s32[384]{0:T(512)} %param.16), channel_id=1, source_target_pairs={{0,2},{2,4},{4,6},{6,8},{8,10},{10,12},{12,14},{14,16},{16,18},{18... | collective-permute-start | bytes 4616 | tf_op jit(solution)/shard_map/ppermute | solution.py:16
  22.8 96.2 %collective-permute-start.8 = (bf16[384,1024]{1,0:T(8,128)(2,1)}, bf16[384,1024]{1,0:T(8,128)(2,1)S(1)}, u32[]{:S(2)}, u32[]{:S(2)}) collective-permute-start(bf16[384,1024]{1,0:T(8,128)(2,1)} %param.13), channel_id=1, source_target_pairs={{0,8},{2,10},{4,12},{6,14},{8,16},{10,18},{12,20},{14,22},{16,24},... | collective-permute-start | bytes 2359304 | tf_op jit(solution)/shard_map/ppermute | solution.py:16
  27.9 103.6 %copy-start.1 = (bf16[384,1024]{1,0:T(8,128)(2,1)S(1)}, bf16[384,1024]{1,0:T(8,128)(2,1)}, u32[]{:S(2)}) copy-start(bf16[384,1024]{1,0:T(8,128)(2,1)} %param.13) | copy-start | bytes 2359300
  27.9 95.1 %collective-permute-start.9 = (bf16[384,1024]{1,0:T(8,128)(2,1)}, bf16[384,1024]{1,0:T(8,128)(2,1)S(1)}, u32[]{:S(2)}, u32[]{:S(2)}) collective-permute-start(bf16[384,1024]{1,0:T(8,128)(2,1)} %param.13), channel_id=1, source_target_pairs={{0,6},{2,8},{4,10},{6,12},{8,14},{10,16},{12,18},{14,20},{16,22},{... | collective-permute-start | bytes 2359304 | tf_op jit(solution)/shard_map/ppermute | solution.py:16
  31.8 94.9 %collective-permute-start.10 = (bf16[384,1024]{1,0:T(8,128)(2,1)}, bf16[384,1024]{1,0:T(8,128)(2,1)S(1)}, u32[]{:S(2)}, u32[]{:S(2)}) collective-permute-start(bf16[384,1024]{1,0:T(8,128)(2,1)} %param.13), channel_id=1, source_target_pairs={{0,4},{2,6},{4,8},{6,10},{8,12},{10,14},{12,16},{14,18},{16,20},{1... | collective-permute-start | bytes 2359304 | tf_op jit(solution)/shard_map/ppermute | solution.py:16
  35.3 95.2 %collective-permute-start.11 = (bf16[384,1024]{1,0:T(8,128)(2,1)}, bf16[384,1024]{1,0:T(8,128)(2,1)S(1)}, u32[]{:S(2)}, u32[]{:S(2)}) collective-permute-start(bf16[384,1024]{1,0:T(8,128)(2,1)} %param.13), channel_id=1, source_target_pairs={{0,2},{2,4},{4,6},{6,8},{8,10},{10,12},{12,14},{14,16},{16,18},{18... | collective-permute-start | bytes 2359304 | tf_op jit(solution)/shard_map/ppermute | solution.py:16
  36.6 6.0 collective-permute-start.12
  42.7 56.3 %collective-permute-start.13 = (f32[384,16]{0,1:T(8,128)}, f32[384,16]{0,1:T(8,128)S(1)}, u32[]{:S(2)}, u32[]{:S(2)}) collective-permute-start(f32[384,16]{0,1:T(8,128)} %param.15), channel_id=1, source_target_pairs={{0,6},{2,8},{4,10},{6,12},{8,14},{10,16},{12,18},{14,20},{16,22},{... | collective-permute-start | bytes 73736 | tf_op jit(solution)/shard_map/ppermute | solution.py:16
  99.0 3.0 collective-permute-start.14
  102.0 8.0 %collective-permute-start.15 = (f32[384,16]{0,1:T(8,128)}, f32[384,16]{0,1:T(8,128)S(1)}, u32[]{:S(2)}, u32[]{:S(2)}) collective-permute-start(f32[384,16]{0,1:T(8,128)} %param.15), channel_id=1, source_target_pairs={{0,2},{2,4},{4,6},{6,8},{8,10},{10,12},{12,14},{14,16},{16,18},{18... | collective-permute-start | bytes 73736 | tf_op jit(solution)/shard_map/ppermute | solution.py:16
  110.0 28.7 %collective-permute-start = (bf16[384,1024]{1,0:T(8,128)(2,1)}, bf16[384,1024]{1,0:T(8,128)(2,1)S(1)}, u32[]{:S(2)}, u32[]{:S(2)}) collective-permute-start(bf16[384,1024]{1,0:T(8,128)(2,1)} %param.14), channel_id=1, source_target_pairs={{0,8},{2,10},{4,12},{6,14},{8,16},{10,18},{12,20},{14,22},{16,24},... | collective-permute-start | bytes 2359304 | tf_op jit(solution)/shard_map/ppermute | solution.py:16
  119.0 20.6 %collective-permute-start.1 = (bf16[384,1024]{1,0:T(8,128)(2,1)}, bf16[384,1024]{1,0:T(8,128)(2,1)}, u32[]{:S(2)}, u32[]{:S(2)}) collective-permute-start(bf16[384,1024]{1,0:T(8,128)(2,1)} %param.14), channel_id=1, source_target_pairs={{0,6},{2,8},{4,10},{6,12},{8,14},{10,16},{12,18},{14,20},{16,22},{... | collective-permute-start | bytes 2359304 | tf_op jit(solution)/shard_map/ppermute | solution.py:16
  123.0 30.7 %collective-permute-start.2 = (bf16[384,1024]{1,0:T(8,128)(2,1)S(1)}, bf16[384,1024]{1,0:T(8,128)(2,1)S(1)}, u32[]{:S(2)}, u32[]{:S(2)}) collective-permute-start(bf16[384,1024]{1,0:T(8,128)(2,1)S(1)} %copy-done.2), channel_id=1, source_target_pairs={{0,4},{2,6},{4,8},{6,10},{8,12},{10,14},{12,16},{14,18},{16,20},{1... | collective-permute-start | bytes 2359304 | tf_op jit(solution)/shard_map/ppermute | solution.py:16
  126.8 27.8 %collective-permute-start.3 = (bf16[384,1024]{1,0:T(8,128)(2,1)S(1)}, bf16[384,1024]{1,0:T(8,128)(2,1)}, u32[]{:S(2)}, u32[]{:S(2)}) collective-permute-start(bf16[384,1024]{1,0:T(8,128)(2,1)S(1)} %copy-done.2), channel_id=1, source_target_pairs={{0,2},{2,4},{4,6},{6,8},{8,10},{10,12},{12,14},{14,16},{16,18},{18... | collective-permute-start | bytes 2359304 | tf_op jit(solution)/shard_map/ppermute | solution.py:16
  157.6 6.4 copy-start.3
  157.6 6.4 copy-start.4
  190.9 17.4 %copy-start.5 = (bf16[1024,2048]{1,0:T(8,128)(2,1)S(1)}, bf16[1024,2048]{1,0:T(8,128)(2,1)}, u32[]{:S(2)}) copy-start(bf16[1024,2048]{1,0:T(8,128)(2,1)} %param.17) | copy-start | bytes 12582916
  211.4 45.0 %copy-start = (bf16[384,2048]{1,0:T(8,128)(2,1)S(1)}, bf16[384,2048]{1,0:T(8,128)(2,1)}, u32[]{:S(2)}) copy-start(bf16[384,2048]{1,0:T(8,128)(2,1)} %param.11) | copy-start | bytes 4718596
  211.4 158.9 %copy-start.6 = (f32[2048]{0:T(1024)S(1)}, f32[2048]{0:T(1024)}, u32[]{:S(2)}) copy-start(f32[2048]{0:T(1024)} %param.18) | copy-start | bytes 24580
  211.4 158.9 %all-gather.4.cloned.1.call-start = ((), (), s32[]{:S(2)}) async-start(), calls=%async_computation.2 | async-start | bytes 11141120 | tf_op jit(solution)/shard_map/all_gather | solution.py:88
  212.0 290.3 %all-gather.6.cloned.1.call-start = ((), (), s32[]{:S(2)}) async-start(), calls=%async_computation.3 | async-start | bytes 11141120 | tf_op jit(solution)/shard_map/all_gather | solution.py:89
  212.6 459.0 %all-gather.8.cloned.1.call-start = ((), (), s32[]{:S(2)}) async-start(), calls=%async_computation.4 | async-start | bytes 11141120 | tf_op jit(solution)/shard_map/all_gather | solution.py:96
  213.1 483.5 %reduce-scatter.2.cloned.1.call-start = ((), (), s32[]{:S(2)}) async-start(), calls=%async_computation.5 | async-start | bytes 2359296 | tf_op jit(solution)/shard_map/reduce_scatter | solution.py:99
Sparse Core Ops, SparseCore 0:
  211.5 44.7 all-reduce.1
  689.4 7.2 reduce-scatter.1
Sparse Core Ops, SparseCore 1:
  214.6 155.6 all-gather.3
  372.8 129.4 all-gather.5
  504.9 166.6 all-gather.7
where the time goes:
time: 708 us; the launch traced here: 707 us
  waiting for transfers between devices  473 us (67%)
  starting transfers between devices  109 us (15%)
  matrix products  73.9 us (10%)
  local copies, waits for them, and re-layouts  27.4 us (4%)
  between operations  15.3 us (2%)
  other arithmetic  7.69 us (1%)
    all_gather x1, waiting for transfers between devices, local(): lax.all_gather(down_weight, 'sp', axis=1, tiled=True)  169 us
    all_gather x1, waiting for transfers between devices, local(): lax.all_gather(up_weight, 'sp', axis=0, tiled=True)  123 us
    all_gather x1, waiting for transfers between devices, local(): lax.all_gather(gate_weight, 'sp', axis=0, tiled=True)  112 us
    ppermute x16, starting transfers between devices, from_behind(): lax.ppermute(value, axis, [(source, source + steps) for source in range(f...  108 us
    psum x1, waiting for transfers between devices, local(): lax.psum(partial_value.astype(jnp.bfloat16), 'tp').astype(jnp.float32)  43 us
    sub x1, matrix products, local(): exp_scores = jnp.exp(scores - row_max)  26.9 us
    dot_general x1, matrix products, local(): jnp.dot(hidden, lax.all_gather(down_weight, 'sp', axis=1, tiled=True), pr...  17.7 us
    dot_general x1, matrix products, local(): jnp.einsum('hqk,khd->qhd', weights, value_heads, preferred_element_type=j...  17.4 us
  transfers between devices with their start and end apart: 21, of which 10 were waited for; matrix products, arithmetic and copies ran while one was open for 5% of the time, Pallas kernels for 0%

commit v1 on v0

--- a/solution.py
+++ b/solution.py
@@ -1,6 +1,10 @@
+import functools
+
 import jax
 import jax.numpy as jnp
 from jax import lax
+from jax.experimental import pallas as pl
+from jax.experimental.pallas import tpu as pltpu
 from jax.sharding import PartitionSpec as P
 
 REACH = 4
@@ -22,7 +26,7 @@
     return (widened * factor * gain).astype(jnp.bfloat16)
 
 
-def local(
+def plain_local(
     residual,
     queries,
     keys,
@@ -102,9 +106,291 @@
     return (middle.astype(jnp.float32) + down_sum).astype(jnp.bfloat16)
 
 
+ROWS = 128
+
+
+def attend_tile(tile, plane_index, span, head_size, queries, keys, values, aux, out):
+    heads = queries.shape[1] // head_size
+    q_start = pl.multiple_of(tile * ROWS, ROWS)
+    window = span + ROWS
+    key_aux = aux[:, pl.ds(q_start, window)]
+    query_aux = jnp.transpose(aux[:, pl.ds(pl.multiple_of(q_start + span, ROWS), ROWS)])
+    column = lax.broadcasted_iota(jnp.int32, (ROWS, window), 1)
+    row = lax.broadcasted_iota(jnp.int32, (ROWS, window), 0)
+    first = (1 - plane_index) * span - q_start
+    visible = (
+        (column <= row + span)
+        & (column >= first)
+        & (key_aux[heads : heads + 1, :] == query_aux[:, heads : heads + 1])
+    )
+    query = queries[pl.ds(q_start, ROWS), :] * jnp.bfloat16(head_size ** (-0.5))
+    parts = []
+    for head in range(heads):
+        lanes = slice(head * head_size, (head + 1) * head_size)
+        key = keys[pl.ds(q_start, window), lanes]
+        scores = lax.dot_general(
+            query[:, lanes], key, (((1,), (1,)), ((), ())), preferred_element_type=jnp.float32
+        )
+        scores = scores + (query_aux[:, head : head + 1] - key_aux[head : head + 1, :])
+        scores = jnp.where(visible, scores, NEGATIVE)
+        exp_scores = jnp.exp(scores - jnp.max(scores, axis=-1, keepdims=True))
+        total = jnp.sum(exp_scores, axis=-1, keepdims=True)
+        mixed = jnp.dot(
+            exp_scores.astype(jnp.bfloat16),
+            values[pl.ds(q_start, window), lanes],
+            preferred_element_type=jnp.float32,
+        )
+        parts.append(mixed / total)
+    out[pl.ds(q_start, ROWS), :] = jnp.concatenate(parts, axis=1).astype(jnp.bfloat16)
+
+
+def attend_kernel(
+    planes, group, head_size,
+    queries, keys, values, aux, gate, up, down,
+    attended, gate_all, up_all, down_all,
+    q_buf, k_buf, v_buf, aux_buf, out_buf,
+    a_send, a_recv, a_own, h_send, h_recv, w_send, w_recv, g_send, g_recv, w_own, b_send, b_recv, b_own,
+):
+    me = lax.axis_index("sp")
+    plane, place = me // group, lax.rem(me, group)
+    tok = queries.shape[0]
+    cols = queries.shape[1] // group
+    span = tok * group
+    depth = gate.shape[0]
+    width = gate.shape[1] // planes
+    MESH = pl.DeviceIdType.MESH
+
+    def neighbour(step):
+        return lax.rem(place + step, group)
+
+    def in_plane(step):
+        return {"sp": plane * group + neighbour(step)}
+
+    def other_plane(step):
+        return lax.rem(plane + step, planes)
+
+    def across(step):
+        return {"sp": other_plane(step) * group + place}
+
+    barrier = pltpu.get_barrier_semaphore()
+    for step in range(1, group):
+        pl.semaphore_signal(barrier, inc=1, device_id=in_plane(step), device_id_type=MESH)
+    for step in range(1, planes):
+        pl.semaphore_signal(barrier, inc=1, device_id=across(step), device_id_type=MESH)
+    pl.semaphore_wait(barrier, group + planes - 2)
+
+    def remote(src, dst, send, recv, device):
+        return pltpu.make_async_remote_copy(
+            src_ref=src, dst_ref=dst, send_sem=send, recv_sem=recv,
+            device_id=device, device_id_type=MESH,
+        )
+
+    own_rows = pl.ds(pl.multiple_of(span + place * tok, 128), tok)
+    q_rows = pl.ds(pl.multiple_of(place * tok, 128), tok)
+
+    def head_cols(index):
+        return pl.ds(pl.multiple_of(index * cols, 128), cols)
+
+    spread = []
+    for step in range(1, group):
+        to = neighbour(step)
+        for i, (src, dst, rows) in enumerate(
+            ((keys, k_buf, own_rows), (values, v_buf, own_rows), (queries, q_buf, q_rows))
+        ):
+            spread.append(remote(src.at[:, head_cols(to)], dst.at[rows, :],
+                                 a_send.at[i, step], a_recv.at[i, step], in_plane(step)))
+        spread.append(remote(aux.at[to], aux_buf.at[:, own_rows],
+                             a_send.at[3, step], a_recv.at[3, step], in_plane(step)))
+    own = [
+        pltpu.make_async_copy(keys.at[:, head_cols(place)], k_buf.at[own_rows, :], a_own.at[0]),
+        pltpu.make_async_copy(values.at[:, head_cols(place)], v_buf.at[own_rows, :], a_own.at[1]),
+        pltpu.make_async_copy(queries.at[:, head_cols(place)], q_buf.at[q_rows, :], a_own.at[2]),
+        pltpu.make_async_copy(aux.at[place], aux_buf.at[:, own_rows], a_own.at[3]),
+    ]
+    for copy in spread + own:
+        copy.start()
+
+    def piece(m, part):
+        at = pl.ds(pl.multiple_of(part * width, 128), width)
+        return down.at[at, :] if m == 2 else (gate, up)[m].at[:, at]
+
+    def slot(m, source_plane):
+        at = pl.ds(pl.multiple_of((source_plane * group + place) * depth, 128), depth)
+        return down_all.at[:, at] if m == 2 else (gate_all, up_all)[m].at[at, :]
+
+    first = {
+        (m, step): remote(piece(m, other_plane(step)), slot(m, plane),
+                          w_send.at[m, step], w_recv.at[m, step], across(step))
+        for m in range(3) for step in range(1, planes)
+    }
+    second = {}
+    kept = [pltpu.make_async_copy(piece(m, plane), slot(m, plane), w_own.at[m]) for m in range(3)]
+    for copy in kept:
+        copy.start()
+
+    def forward(m, source_step):
+        source = lax.rem(plane + planes - source_step, planes)
+        for step in range(1, group):
+            src = piece(m, plane) if source_step == 0 else slot(m, source)
+            copy = remote(src, slot(m, source), g_send.at[m, source_step, step],
+                          g_recv.at[m, source_step, step], in_plane(step))
+            copy.start()
+            second[m, source_step, step] = copy
+
+    for step in range(1, planes):
+        first[0, step].start()
+    for copy in own:
+        copy.wait()
+    for copy in spread:
+        copy.wait()
+    late, early = pl.ds(span, span), pl.ds(0, span)
+    halo = [
+        remote(k_buf.at[late, :], k_buf.at[early, :], h_send.at[0], h_recv.at[0], across(1)),
+        remote(v_buf.at[late, :], v_buf.at[early, :], h_send.at[1], h_recv.at[1], across(1)),
+        remote(aux_buf.at[:, late], aux_buf.at[:, early], h_send.at[2], h_recv.at[2], across(1)),
+    ]
+    for copy in halo:
+        copy.start()
+    for m in range(1, 3):
+        for step in range(1, planes):
+            first[m, step].start()
+    for m in range(3):
+        forward(m, 0)
+    for m in range(3):
+        for step in range(1, planes):
+            first[m, step].wait()
+            forward(m, step)
+    for copy in halo:
+        copy.wait()
+
+    def one(tile, carry):
+        attend_tile(tile, plane, span, head_size, q_buf, k_buf, v_buf, aux_buf, out_buf)
+        return carry
+
+    lax.fori_loop(0, span // ROWS, one, 0)
+
+    back = []
+    for step in range(1, group):
+        rows = pl.ds(pl.multiple_of(neighbour(step) * tok, 128), tok)
+        back.append(remote(out_buf.at[rows, :], attended.at[:, head_cols(place)],
+                           b_send.at[step], b_recv.at[step], in_plane(step)))
+    stay = pltpu.make_async_copy(out_buf.at[q_rows, :], attended.at[:, head_cols(place)], b_own)
+    for copy in back:
+        copy.start()
+    stay.start()
+    stay.wait()
+    for copy in back + kept:
+        copy.wait()
+    for copy in second.values():
+        copy.wait()
+
+
+def attend_and_gather(queries, keys, values, aux, gate, up, down, planes, group, head_size):
+    tok, all_cols = queries.shape
+    cols, span = all_cols // group, tok * group
+    features, width = gate.shape[0] * planes * group, gate.shape[1] // planes
+    sem = pltpu.SemaphoreType.DMA
+    anywhere = pl.BlockSpec(memory_space=pl.ANY)
+    bf16 = jnp.bfloat16
+    return pl.pallas_call(
+        functools.partial(attend_kernel, planes, group, head_size),
+        out_shape=(
+            jax.ShapeDtypeStruct((tok, all_cols), bf16),
+            jax.ShapeDtypeStruct((features, width), bf16),
+            jax.ShapeDtypeStruct((features, width), bf16),
+            jax.ShapeDtypeStruct((width, features), bf16),
+        ),
+        in_specs=[anywhere] * 7,
+        out_specs=(anywhere,) * 4,
+        scratch_shapes=[
+            pltpu.VMEM((span, cols), bf16),
+            pltpu.VMEM((2 * span, cols), bf16),
+            pltpu.VMEM((2 * span, cols), bf16),
+            pltpu.VMEM((8, 2 * span), jnp.float32),
+            pltpu.VMEM((span, cols), bf16),
+            sem((4, group)), sem((4, group)), sem((4,)),
+            sem((3,)), sem((3,)),
+            sem((3, planes)), sem((3, planes)),
+            sem((3, planes, group)), sem((3, planes, group)),
+            sem((3,)),
+            sem((group,)), sem((group,)), sem,
+        ],
+        compiler_params=pltpu.CompilerParams(
+            collective_id=0, has_side_effects=True, vmem_limit_bytes=40 * 1024 * 1024
+        ),
+    )(queries, keys, values, aux, gate, up, down)
+
+
+def grouped_local(
+    planes, group,
+    residual, queries, keys, values, gate_cache, doc_ids,
+    out_weight, mix_gain, gate_weight, up_weight, down_weight,
+):
+    tok_rows = queries.shape[0]
+    heads_here = gate_cache.shape[1]
+    head_size = queries.shape[1] // heads_here
+    heads = heads_here // group
+    rows = gate_cache.T.reshape(group, heads, tok_rows)
+    docs = jnp.broadcast_to(doc_ids.astype(jnp.float32), (group, 1, tok_rows))
+    fill = jnp.zeros((group, 7 - heads, tok_rows), jnp.float32)
+    aux = jnp.concatenate([rows, docs, fill], axis=1)
+    attended, gate, up, down = attend_and_gather(
+        queries, keys, values, aux, gate_weight, up_weight, down_weight, planes, group, head_size
+    )
+    tp_count = lax.axis_size("tp")
+    row_share = tok_rows // tp_count
+    tp_index = lax.axis_index("tp")
+    partial_value = jnp.dot(attended, out_weight, preferred_element_type=jnp.float32)
+    return finish(
+        planes, group, residual, partial_value.astype(jnp.bfloat16), mix_gain, gate, up, down,
+        row_share, tp_index,
+    )
+
+
+def finish(planes, group, residual, partial_value, mix_gain, gate, up, down, row_share, tp_index):
+    peers = [[plane * group + place for plane in range(planes)] for place in range(group)]
+    attn_sum = lax.psum(partial_value, "tp").astype(jnp.float32)
+    whole_middle = (residual.astype(jnp.float32) + attn_sum).astype(jnp.bfloat16)
+    mixer_in = normalize(whole_middle, mix_gain)
+    middle = lax.dynamic_slice_in_dim(whole_middle, tp_index * row_share, row_share, 0)
+    tokens = lax.all_gather(mixer_in, "sp", axis=0, tiled=True, axis_index_groups=peers)
+    gate_proj = jnp.dot(tokens, gate, preferred_element_type=jnp.float32)
+    up_proj = jnp.dot(tokens, up, preferred_element_type=jnp.float32)
+    hidden = (jax.nn.silu(gate_proj) * up_proj).astype(jnp.bfloat16)
+    partials = jnp.dot(hidden, down, preferred_element_type=jnp.float32).astype(jnp.bfloat16)
+    mine = lax.psum_scatter(
+        partials, "sp", scatter_dimension=0, tiled=True, axis_index_groups=peers
+    )
+    down_sum = lax.psum_scatter(mine, "tp", scatter_dimension=0, tiled=True).astype(jnp.float32)
+    return (middle.astype(jnp.float32) + down_sum).astype(jnp.bfloat16)
+
+
+def choose(
+    residual, queries, keys, values, gate_cache, doc_ids,
+    out_weight, mix_gain, gate_weight, up_weight, down_weight,
+):
+    arrays = (
+        residual, queries, keys, values, gate_cache, doc_ids,
+        out_weight, mix_gain, gate_weight, up_weight, down_weight,
+    )
+    count, group = lax.axis_size("sp"), REACH
+    planes = count // group
+    heads = gate_cache.shape[1] // group
+    fits = (
+        count == planes * group
+        and gate_cache.shape[1] == heads * group
+        and 1 <= heads <= 7
+        and queries.shape[0] % 128 == 0
+        and (queries.shape[1] // group) % 128 == 0
+        and gate_weight.shape[0] % 128 == 0
+        and gate_weight.shape[1] % (planes * 128) == 0
+    )
+    return grouped_local(planes, group, *arrays) if fits else plain_local(*arrays)
+
+
 def solution(mesh):
     return jax.shard_map(
-        local,
+        choose,
         mesh=mesh,
         in_specs=(
             P("sp", None),

time: 708 us -> 455 us (0.64)
  waiting for transfers between devices: 473 us -> 259 us
  Pallas kernels: 0 us -> 134 us
  starting transfers between devices: 109 us -> 0.31 us
  matrix products: 73.9 us -> 28.6 us
  local copies, waits for them, and re-layouts: 27.4 us -> 11.7 us
    all_gather x3 -> x1, waiting for transfers between devices: 404 us -> 116 us  [finish(): lax.all_gather(mixer_in, 'sp', axis=0, tiled=True, axis_index_groups=peers)]
    pallas_call x0 -> x1, Pallas kernels: none -> 134 us  [attend_and_gather(): pl.pallas_call(functools.partial(attend_kernel, planes, group, head_size)...]
    reduce_scatter x1 -> x2, waiting for transfers between devices: 7.37 us -> 121 us  [the longest x1 109 us: finish(): lax.psum_scatter(partials, 'sp', scatter_dimension=0, tiled=True, axis_in...]
    ppermute x16 -> x0, starting transfers between devices: 108 us -> none  [from_behind(): lax.ppermute(value, axis, [(source, source + steps) for source in range(f...]
    sub x1 -> x0, matrix products: 26.9 us -> none  [local(): exp_scores = jnp.exp(scores - row_max)]
    psum x1, waiting for transfers between devices: 43 us -> 21.7 us  [finish(): attn_sum = lax.psum(partial_value, 'tp').astype(jnp.float32)]
    dot_general x4 -> x3, matrix products: 47.1 us -> 28.6 us  [the longest x1 16.5 us: finish(): jnp.dot(hidden, down, preferred_element_type=jnp.float32)]
    ppermute x16 -> x0, waiting for transfers between devices: 17.4 us -> none  [from_behind(): lax.ppermute(value, axis, [(source, source + steps) for source in range(f...]
  transfers between devices with their start and end apart: 21 -> 4, of which waited for: 10 -> 4; matrix products, arithmetic and copies ran while one was open for 5% -> 0% of each run, Pallas kernels for 0% -> 0%
where the time goes in v1:
time: 455 us; the launch traced here: 454 us
  waiting for transfers between devices  259 us (57%)
  Pallas kernels  134 us (29%)
  matrix products  28.6 us (6%)
  between operations  13.2 us (3%)
  local copies, waits for them, and re-layouts  11.7 us (3%)
  other arithmetic  7.27 us (2%)
    pallas_call x1, Pallas kernels, attend_and_gather(): pl.pallas_call(functools.partial(attend_kernel, planes, group, head_size)...  134 us
    all_gather x1, waiting for transfers between devices, finish(): lax.all_gather(mixer_in, 'sp', axis=0, tiled=True, axis_index_groups=peers)  116 us
    reduce_scatter x1, waiting for transfers between devices, finish(): lax.psum_scatter(partials, 'sp', scatter_dimension=0, tiled=True, axis_in...  109 us
    psum x1, waiting for transfers between devices, finish(): attn_sum = lax.psum(partial_value, 'tp').astype(jnp.float32)  21.7 us
    dot_general x1, matrix products, finish(): jnp.dot(hidden, down, preferred_element_type=jnp.float32)  16.5 us
    reduce_scatter x1, waiting for transfers between devices, finish(): lax.psum_scatter(mine, 'tp', scatter_dimension=0, tiled=True)  11.6 us
    unnamed x24, local copies, waits for them, and re-layouts  10.8 us
    dot_general x1, matrix products, finish(): gate_proj = jnp.dot(tokens, gate, preferred_element_type=jnp.float32)  9.2 us
  transfers between devices with their start and end apart: 4, of which 4 were waited for; matrix products, arithmetic and copies ran while one was open for 0% of the time, Pallas kernels for 0%

profile of v1, /device:TPU:0, one launch (start us, length us, event | category | flops | bytes accessed | tf_op | source)
XLA Modules:
  0.0 454.0 jit_solution(3224260077571277634)
XLA Ops:
  6.5 0.0 all-reduce.2.cloned.1.call-start
  6.5 0.7 reshape.12
  7.3 0.7 convert_element_type.37
  8.0 0.1 pad.2.clone
  8.1 0.1 maximum_maximum_fusion.aux
  8.1 0.0 copy-start
  8.1 1.1 copy-done
  9.3 0.0 copy-start.1
  9.3 1.1 copy-done.1
  10.4 0.0 copy-start.2
  10.4 1.1 copy-done.2
  11.5 0.0 copy-start.3
  11.5 1.1 copy-done.3
  12.6 0.0 copy-start.4
  12.6 1.1 copy-done.4
  13.7 0.0 copy-start.5
  13.7 1.1 copy-done.5
  14.8 0.0 copy-start.11
  14.8 134.0 %shard_map.109 = (bf16[384,1024]{1,0:T(8,128)(2,1)S(1)}, bf16[2048,640]{1,0:T(8,128)(2,1)S(1)}, bf16[2048,640]{1,0:T(8,128)(2,1)S(1)}, bf16[640,2048]{1,0:T(8,128)(2,1)S(1)}) custom-call(bf16[384,1024]{1,0:T(8,128)(2,1)S(1)} %copy-done, bf16[384,1024]{1,0:T(8,128)(2,1)S(1)} %copy-done.1, bf16[384,1024]{1,0:T(8,128)(2,1)S(1)} %copy-done.2, ...), custom_call_target="tpu_custom_call" | custom-call | tf_op jit(solution)/shard_map/pallas_call | solution.py:295
  148.8 0.0 copy-start.6
  148.8 1.5 copy-done.6
  150.3 0.0 copy-start.7
  150.3 1.5 copy-done.7
  151.9 0.0 copy-done.11
  151.9 2.9 convolution_convert_fusion.1
  154.8 0.0 copy-start.10
  154.8 0.0 all-reduce.2.cloned.1.call-update
  154.9 0.0 all-gather.2.cloned.1.call-start
  154.9 21.7 %all-reduce.2.cloned.1.call-done = bf16[384,2048]{1,0:T(8,128)(2,1)} async-done(((bf16[384,2048]{1,0:T(8,128)(2,1)}), bf16[384,2048]{1,0:T(8,128)(2,1)}) %all-reduce.2.cloned.1.call-update) | async-done | bytes 1572880 | tf_op jit(solution)/shard_map/psum | solution.py:352
  176.6 2.6 fusion
  179.2 0.0 copy-start.8
  179.3 1.1 copy-done.8
  180.4 0.0 copy-done.10
  180.4 1.6 fusion.2
  182.0 0.0 all-gather.2.cloned.1.call-update
  182.0 0.2 reduce-scatter.3.cloned.1.call-start
  182.2 116.4 %all-gather.2.cloned.1.call-done = bf16[1536,2048]{1,0:T(8,128)(2,1)} async-done(((bf16[384,2048]{1,0:T(8,128)(2,1)}), bf16[1536,2048]{1,0:T(8,128)(2,1)}) %all-gather.2.cloned.1.call-update) | async-done | bytes 6291472 | tf_op jit(solution)/shard_map/all_gather | solution.py:356
  298.7 9.2 %fusion.4 = f32[1536,640]{1,0:T(8,128)} fusion(bf16[1536,2048]{1,0:T(8,128)(2,1)} %all-gather.2.cloned.1.call-done, bf16[2048,640]{1,0:T(8,128)(2,1)} %copy-done.7), kind=kOutput, calls=%fused_computation.13 | convolution fusion | flops 4026531840 | bytes 12845056 | tf_op jit(solution)/shard_map/dot_general | solution.py:357
  307.9 16.5 %convolution_convert_fusion = bf16[1536,2048]{1,0:T(8,128)(2,1)} fusion(bf16[640,2048]{1,0:T(8,128)(2,1)} %copy-done.6, f32[1536,640]{1,0:T(8,128)} %fusion.4, bf16[1536,2048]{1,0:T(8,128)(2,1)} %all-gather.2.cloned.1.call-done, bf16[2048,640]{1,0:T(8,128)(2,1)S(1)} %get-tuple-element.11), kind=kOutput, calls=%fused_computation | convolution fusion | flops 8062107648 | bytes 21757952 | tf_op jit(solution)/shard_map/dot_general | solution.py:360
  324.4 0.0 copy-start.9
  324.4 0.0 reduce-scatter.3.cloned.1.call-update
  324.4 0.0 reduce-scatter.5.cloned.1.call-start
  324.4 109.1 %reduce-scatter.3.cloned.1.call-done = bf16[384,2048]{1,0:T(8,128)(2,1)} async-done(((bf16[1536,2048]{1,0:T(8,128)(2,1)}), bf16[384,2048]{1,0:T(8,128)(2,1)}) %reduce-scatter.3.cloned.1.call-update) | async-done | bytes 1572880 | tf_op jit(solution)/shard_map/reduce_scatter | solution.py:361
  433.5 0.0 reduce-scatter.5.cloned.1.call-update
  433.5 11.6 %reduce-scatter.5.cloned.1.call-done = bf16[192,2048]{1,0:T(8,128)(2,1)} async-done(((bf16[384,2048]{1,0:T(8,128)(2,1)}), bf16[192,2048]{1,0:T(8,128)(2,1)}) %reduce-scatter.5.cloned.1.call-update) | async-done | bytes 786448 | tf_op jit(solution)/shard_map/reduce_scatter | solution.py:364
  445.2 0.0 copy-done.9
  445.2 2.3 add_convert_fusion.1
  (3 shorter events, 0.0 us)
Async XLA Ops:
  6.5 170.1 %all-reduce.2.cloned.1.call-start = ((), (), s32[]{:S(2)}) async-start(), calls=%async_computation.2 | async-start | bytes 3145728 | tf_op jit(solution)/shard_map/psum | solution.py:352
  8.1 1.1 copy-start
  9.3 1.1 copy-start.1
  10.4 1.1 copy-start.2
  11.5 1.1 copy-start.3
  12.6 1.1 copy-start.4
  13.7 1.1 copy-start.5
  14.8 137.1 %copy-start.11 = (bf16[1024,2048]{1,0:T(8,128)(2,1)S(1)}, bf16[1024,2048]{1,0:T(8,128)(2,1)}, u32[]{:S(2)}) copy-start(bf16[1024,2048]{1,0:T(8,128)(2,1)} %param.17) | copy-start | bytes 12582916
  148.8 1.5 copy-start.6
  150.3 1.5 copy-start.7
  154.8 25.6 %copy-start.10 = (f32[2048]{0:T(1024)S(1)}, f32[2048]{0:T(1024)}, u32[]{:S(2)}) copy-start(f32[2048]{0:T(1024)} %param.18) | copy-start | bytes 24580
  154.9 143.8 %all-gather.2.cloned.1.call-start = ((), (), s32[]{:S(2)}) async-start(), calls=%async_computation.3 | async-start | bytes 7864320 | tf_op jit(solution)/shard_map/all_gather | solution.py:356
  179.2 1.1 copy-start.8
  182.0 251.5 %reduce-scatter.3.cloned.1.call-start = ((), (), s32[]{:S(2)}) async-start(), calls=%async_computation.4 | async-start | bytes 7864320 | tf_op jit(solution)/shard_map/reduce_scatter | solution.py:361
  324.4 120.8 %copy-start.9 = (bf16[384,2048]{1,0:T(8,128)(2,1)S(1)}, bf16[384,2048]{1,0:T(8,128)(2,1)}, u32[]{:S(2)}) copy-start(bf16[384,2048]{1,0:T(8,128)(2,1)} %copy-done.8) | copy-start | bytes 4718596
  324.4 120.8 %reduce-scatter.5.cloned.1.call-start = ((), (), s32[]{:S(2)}) async-start(), calls=%async_computation.5 | async-start | bytes 2359296 | tf_op jit(solution)/shard_map/reduce_scatter | solution.py:364
Sparse Core Ops, SparseCore 0:
  155.0 21.6 all-reduce.1
  182.1 116.4 all-gather.1
  324.5 108.9 reduce-scatter.2
  435.6 9.5 reduce-scatter.4

commit v2 on v1

--- a/solution.py
+++ b/solution.py
@@ -347,22 +347,120 @@
     )
 
 
+def mix_kernel(
+    planes, group,
+    partial, residual, gain, gate, up, down, out,
+    got, tokens, part, pair, sums, inbox, mid,
+    x_send, x_recv, n_send, n_recv, z_send, z_recv, p_send, p_recv, r_send, r_recv,
+):
+    me, core = lax.axis_index("sp"), lax.axis_index("tp")
+    plane, place = me // group, lax.rem(me, group)
+    half, features = mid.shape
+    other = 1 - core
+    partner = {"tp": other}
+    MESH = pl.DeviceIdType.MESH
+
+    def across(step):
+        return {"sp": lax.rem(plane + step, planes) * group + place}
+
+    barrier = pltpu.get_barrier_semaphore()
+    pl.semaphore_signal(barrier, inc=1, device_id=partner, device_id_type=MESH)
+    for step in range(1, planes):
+        pl.semaphore_signal(barrier, inc=1, device_id=across(step), device_id_type=MESH)
+    pl.semaphore_wait(barrier, planes)
+
+    def remote(src, dst, send, recv, device):
+        copy = pltpu.make_async_remote_copy(
+            src_ref=src, dst_ref=dst, send_sem=send, recv_sem=recv,
+            device_id=device, device_id_type=MESH,
+        )
+        copy.start()
+        return copy
+
+    theirs = pl.ds(pl.multiple_of(other * half, 32), half)
+    remote(partial.at[theirs, :], got, x_send, x_recv, partner).wait()
+    chunk = 32
+
+    def middle_rows(i, carry):
+        at = pl.ds(pl.multiple_of(i * chunk, chunk), chunk)
+        full = pl.ds(pl.multiple_of(core * half + i * chunk, chunk), chunk)
+        total = partial[full, :].astype(jnp.float32) + got[at, :].astype(jnp.float32)
+        middle = (residual[full, :].astype(jnp.float32) + total).astype(jnp.bfloat16)
+        mid[at, :] = middle
+        tokens[plane, core, at, :] = normalize(middle, gain[...])
+        return carry
+
+    lax.fori_loop(0, half // chunk, middle_rows, 0)
+    mine = tokens.at[plane, core]
+    near = [remote(mine, mine, n_send.at[0], n_recv.at[0], partner)]
+    far = [None] + [
+        remote(mine, mine, z_send.at[e], z_recv.at[e], across(e)) for e in range(1, planes)
+    ]
+    pairs, back = [], [None]
+    for e in range(planes):
+        source = lax.rem(plane + planes - e, planes)
+        if e > 0:
+            far[e].wait_recv()
+            held = tokens.at[source, core]
+            near.append(remote(held, held, n_send.at[e], n_recv.at[e], partner))
+        near[e].wait_recv()
+        block = tokens[source].reshape(2 * half, features)
+        gate_proj = jnp.dot(block, gate[...], preferred_element_type=jnp.float32)
+        up_proj = jnp.dot(block, up[...], preferred_element_type=jnp.float32)
+        hidden = (gate_proj / (1.0 + jnp.exp(-gate_proj)) * up_proj).astype(jnp.bfloat16)
+        lowered = jnp.dot(hidden, down[...], preferred_element_type=jnp.float32)
+        part[source] = lowered.astype(jnp.bfloat16).reshape(2, half, features)
+        pairs.append(remote(part.at[source, other], pair.at[source],
+                            p_send.at[e], p_recv.at[e], partner))
+        if e > 0:
+            pairs[e].wait_recv()
+            both = part[source, core].astype(jnp.float32) + pair[source].astype(jnp.float32)
+            sums[source] = both.astype(jnp.bfloat16)
+            back.append(remote(sums.at[source], inbox.at[e],
+                               r_send.at[e], r_recv.at[e], across(planes - e)))
+    pairs[0].wait_recv()
+    for e in range(1, planes):
+        back[e].wait_recv()
+
+    def last_rows(i, carry):
+        at = pl.ds(pl.multiple_of(i * chunk, chunk), chunk)
+        total = part[plane, core, at, :].astype(jnp.float32)
+        total = total + pair[plane, at, :].astype(jnp.float32)
+        for e in range(1, planes):
+            total = total + inbox[e, at, :].astype(jnp.float32)
+        out[at, :] = (mid[at, :].astype(jnp.float32) + total).astype(jnp.bfloat16)
+        return carry
+
+    lax.fori_loop(0, half // chunk, last_rows, 0)
+    for copy in near + far[1:] + pairs + back[1:]:
+        copy.wait_send()
+
+
 def finish(planes, group, residual, partial_value, mix_gain, gate, up, down, row_share, tp_index):
-    peers = [[plane * group + place for plane in range(planes)] for place in range(group)]
-    attn_sum = lax.psum(partial_value, "tp").astype(jnp.float32)
-    whole_middle = (residual.astype(jnp.float32) + attn_sum).astype(jnp.bfloat16)
-    mixer_in = normalize(whole_middle, mix_gain)
-    middle = lax.dynamic_slice_in_dim(whole_middle, tp_index * row_share, row_share, 0)
-    tokens = lax.all_gather(mixer_in, "sp", axis=0, tiled=True, axis_index_groups=peers)
-    gate_proj = jnp.dot(tokens, gate, preferred_element_type=jnp.float32)
-    up_proj = jnp.dot(tokens, up, preferred_element_type=jnp.float32)
-    hidden = (jax.nn.silu(gate_proj) * up_proj).astype(jnp.bfloat16)
-    partials = jnp.dot(hidden, down, preferred_element_type=jnp.float32).astype(jnp.bfloat16)
-    mine = lax.psum_scatter(
-        partials, "sp", scatter_dimension=0, tiled=True, axis_index_groups=peers
-    )
-    down_sum = lax.psum_scatter(mine, "tp", scatter_dimension=0, tiled=True).astype(jnp.float32)
-    return (middle.astype(jnp.float32) + down_sum).astype(jnp.bfloat16)
+    features = residual.shape[1]
+    sem = pltpu.SemaphoreType.DMA
+    local_spec = pl.BlockSpec(memory_space=pltpu.VMEM)
+    bf16 = jnp.bfloat16
+    several = sem((planes,))
+    return pl.pallas_call(
+        functools.partial(mix_kernel, planes, group),
+        out_shape=jax.ShapeDtypeStruct((row_share, features), bf16),
+        in_specs=[local_spec] * 6,
+        out_specs=local_spec,
+        scratch_shapes=[
+            pltpu.VMEM((row_share, features), bf16),
+            pltpu.VMEM((planes, 2, row_share, features), bf16),
+            pltpu.VMEM((planes, 2, row_share, features), bf16),
+            pltpu.VMEM((planes, row_share, features), bf16),
+            pltpu.VMEM((planes, row_share, features), bf16),
+            pltpu.VMEM((planes, row_share, features), bf16),
+            pltpu.VMEM((row_share, features), bf16),
+            sem, sem, several, several, several, several, several, several, several, several,
+        ],
+        compiler_params=pltpu.CompilerParams(
+            collective_id=1, has_side_effects=True, vmem_limit_bytes=58 * 1024 * 1024
+        ),
+    )(partial_value, residual, mix_gain.reshape(1, features), gate, up, down)
 
 
 def choose(
@@ -378,6 +476,8 @@
     heads = gate_cache.shape[1] // group
     fits = (
         count == planes * group
+        and lax.axis_size("tp") == 2
+        and queries.shape[0] % 64 == 0
         and gate_cache.shape[1] == heads * group
         and 1 <= heads <= 7
         and queries.shape[0] % 128 == 0

time: 455 us -> 314 us (0.69)
  waiting for transfers between devices: 259 us -> 0 us
  Pallas kernels: 134 us -> 295 us
  matrix products: 28.6 us -> 3.04 us
  between operations: 13.2 us -> 0.04 us
  other arithmetic: 7.27 us -> 0.76 us
    pallas_call x0 -> x1, Pallas kernels: none -> 161 us  [finish(): pl.pallas_call(functools.partial(mix_kernel, planes, group), out_shape=ja...]
    reduce_scatter x2 -> x0, waiting for transfers between devices: 121 us -> none  [the longest x1 109 us: finish(): lax.psum_scatter(partials, 'sp', scatter_dimension=0, tiled=True, axis_in...]
    all_gather x1 -> x0, waiting for transfers between devices: 116 us -> none  [finish(): lax.all_gather(mixer_in, 'sp', axis=0, tiled=True, axis_index_groups=peers)]
    dot_general x2 -> x0, matrix products: 25.7 us -> none  [the longest x1 16.5 us: finish(): jnp.dot(hidden, down, preferred_element_type=jnp.float32)]
    psum x1 -> x0, waiting for transfers between devices: 21.7 us -> none  [finish(): attn_sum = lax.psum(partial_value, 'tp').astype(jnp.float32)]
    unnamed x24 -> x21, local copies, waits for them, and re-layouts: 10.8 us -> 13.3 us
  transfers between devices with their start and end apart: 4 -> 0, of which waited for: 4 -> 0; matrix products, arithmetic and copies ran while one was open for 0% -> 0% of each run, Pallas kernels for 0% -> 0%
where the time goes in v2:
time: 314 us; the launch traced here: 313 us
  Pallas kernels  295 us (94%)
  local copies, waits for them, and re-layouts  14.1 us (4%)
    pallas_call x1, Pallas kernels, finish(): pl.pallas_call(functools.partial(mix_kernel, planes, group), out_shape=ja...  161 us
    pallas_call x1, Pallas kernels, attend_and_gather(): pl.pallas_call(functools.partial(attend_kernel, planes, group, head_size)...  134 us
    unnamed x21, local copies, waits for them, and re-layouts  13.3 us

profile of v2, /device:TPU:0, one launch (start us, length us, event | category | flops | bytes accessed | tf_op | source)
XLA Modules:
  0.0 313.3 jit_solution(6663972897553650488)
XLA Ops:
  0.0 0.1 pad.2.clone
  0.1 0.7 convert_element_type.6
  0.8 0.7 reshape.6
  1.5 0.1 maximum_maximum_fusion.aux
  1.6 0.0 copy-start.3
  1.6 1.1 copy-done.3
  2.7 0.0 copy-start.4
  2.7 1.1 copy-done.4
  3.9 0.0 copy-start.5
  3.9 1.1 copy-done.5
  5.0 0.0 copy-start.6
  5.0 1.1 copy-done.6
  6.1 0.0 copy-start.7
  6.1 1.1 copy-done.7
  7.2 0.0 copy-start.8
  7.2 1.1 copy-done.8
  8.3 0.0 copy-start.9
  8.3 134.0 %shard_map.109 = (bf16[384,1024]{1,0:T(8,128)(2,1)S(1)}, bf16[2048,640]{1,0:T(8,128)(2,1)S(1)}, bf16[2048,640]{1,0:T(8,128)(2,1)S(1)}, bf16[640,2048]{1,0:T(8,128)(2,1)S(1)}) custom-call(bf16[384,1024]{1,0:T(8,128)(2,1)S(1)} %copy-done.3, bf16[384,1024]{1,0:T(8,128)(2,1)S(1)} %copy-done.4, bf16[384,1024]{1,0:T(8,128)(2,1)S(1)} %copy-done.5, ...), custom_call_target="tpu_custom_call" | custom-call | tf_op jit(solution)/shard_map/pallas_call | solution.py:295
  142.3 0.0 copy-start
  142.3 1.5 copy-done
  143.8 0.0 copy-start.1
  143.8 1.5 copy-done.1
  145.3 0.0 copy-start.2
  145.3 1.5 copy-done.2
  146.8 0.0 copy-done.9
  146.8 3.0 convolution_convert_fusion.partial
  149.9 161.3 %shard_map.110 = bf16[192,2048]{1,0:T(8,128)(2,1)} custom-call(bf16[384,2048]{1,0:T(8,128)(2,1)} %convolution_convert_fusion.partial, bf16[384,2048]{1,0:T(8,128)(2,1)} %residual.1, f32[1,2048]{1,0:T(1,128)} %bitcast.5, bf16[2048,640]{1,0:T(8,128)(2,1)} %copy-done, bf16[2048,640]{1,0:T(8,128)(2,1)} %copy-done.1, bf16[640,2048]{1,0:T(8,128)(2,1)} %copy-done.2), custom_call_target="tpu_custom_call" | custom-call | tf_op jit(solution)/shard_map/pallas_call | solution.py:445
  311.2 2.1 copy.13
  (2 shorter events, 0.0 us)
Async XLA Ops:
  1.6 1.1 copy-start.3
  2.7 1.1 copy-start.4
  3.9 1.1 copy-start.5
  5.0 1.1 copy-start.6
  6.1 1.1 copy-start.7
  7.2 1.1 copy-start.8
  8.3 138.6 %copy-start.9 = (bf16[1024,2048]{1,0:T(8,128)(2,1)S(1)}, bf16[1024,2048]{1,0:T(8,128)(2,1)}, u32[]{:S(2)}) copy-start(bf16[1024,2048]{1,0:T(8,128)(2,1)} %param.17) | copy-start | bytes 12582916
  142.3 1.5 copy-start
  143.8 1.5 copy-start.1
  145.3 1.5 copy-start.2
